TPU v7x, 32 devices: a whole 2x2x4 slice. The times are simulated.
32 devices in a mesh: sp: 8 (over z, y), tp: 4 (over x, core).
Axes of the slice: x: 2, y: 2, z: 4, core: 2. Of those that a mesh axis runs over, the one named last changes fastest.
Arguments:
- tokens: bfloat16 [1024, 2048], P(('sp', 'tp')), may hold values from -64 to 64, as said below
- query_one: bfloat16 [2048, 256], P(None, 'tp'), may hold values from -0.125 to 0.125
- query_two: bfloat16 [2048, 256], P(None, 'tp'), may hold values from -0.125 to 0.125
- key_one: bfloat16 [2048, 256], P(None, 'tp'), may hold values from -0.125 to 0.125
- key_two: bfloat16 [2048, 256], P(None, 'tp'), may hold values from -0.125 to 0.125
- value_weight: bfloat16 [2048, 512], P(None, 'tp'), may hold values from -0.125 to 0.125
- mixing: float32 [4], P('tp'), may hold values from 0.3 to 0.8
- out_weight: bfloat16 [512, 2048], replicated, may hold values from -0.25 to 0.25
- head_gain: float32 [128], replicated, may hold values from 0.1 to 1.9
Outputs:
- attended: bfloat16 [1024, 2048], P(('sp', 'tp'))
Inputs may be any that keep to these rules, and one draw needn't show every extreme that they name: `tokens`: Real-valued activations.
All inputs are finite; a program needn't handle non-finite values.
Results may differ from a plain program's by a relative error of at most 0.012.
The roundings to bfloat16 on the way count: a program that leaves them out, or rounds other values in their place, can miss the bound.
Values may be sent and summed in bfloat16 or wider, within the bound.
No kernel may reach another device: no remote copies, remote signals or barrier semaphores. Data moves between devices by JAX's collectives and lax.ppermute only.
A program may use at most 64 MiB of HBM per device.

v0:
```python
import math
import jax
import jax.numpy as jnp
from jax import lax
from jax.sharding import PartitionSpec as P

HEAD = 64
GRID_W = 64
epsilon = 1e-06
theta_base = 10000.0
floor_value = -1e30


def grid_turn(field, positions):
    quarter = field.shape[-1] // 4
    half = 2 * quarter
    freqs = theta_base ** (-jnp.arange(quarter, dtype=jnp.float32) / quarter)
    row_angle = (positions // GRID_W).astype(jnp.float32)[:, None] * freqs
    col_angle = (positions % GRID_W).astype(jnp.float32)[:, None] * freqs

    def turn(segment, angle):
        cosine = jnp.cos(angle)[:, None, :]
        sine = jnp.sin(angle)[:, None, :]
        first = segment[..., :quarter]
        second = segment[..., quarter:]
        return jnp.concatenate(
            [first * cosine - second * sine, first * sine + second * cosine], axis=-1
        )

    return jnp.concatenate(
        [turn(field[..., :half], row_angle), turn(field[..., half:], col_angle)], axis=-1
    )


def one_map(state, queries, keys, values):
    peak, total, summed = state
    scores = jnp.einsum(
        "qhd,khd->qhk", queries, keys, preferred_element_type=jnp.float32
    ) * HEAD ** (-0.5)
    new_peak = jnp.maximum(peak, jnp.max(scores, axis=-1))
    factor = jnp.exp(peak - new_peak)
    weights = jnp.exp(scores - new_peak[..., None])
    total = total * factor + jnp.sum(weights, axis=-1)
    summed = summed * factor[..., None] + jnp.einsum(
        "qhk,khe->qhe", weights.astype(jnp.bfloat16), values, preferred_element_type=jnp.float32
    )
    return (new_peak, total, summed)


def make_absorb(q_first, q_second, head_local):
    cols = head_local * HEAD

    def absorb(carry, piece, start):
        count = piece.shape[0]
        width = math.gcd(count, 2048)

        def step(index, state):
            block = lax.dynamic_slice_in_dim(piece, index * width, width, 0)
            keys_first = block[:, :cols].reshape(width, head_local, HEAD)
            keys_second = block[:, cols : 2 * cols].reshape(width, head_local, HEAD)
            values = block[:, 2 * cols :].reshape(width, head_local, 2 * HEAD)
            return (
                one_map(state[0], q_first, keys_first, values),
                one_map(state[1], q_second, keys_second, values),
            )

        return lax.fori_loop(0, count // width, step, carry)

    return absorb


def per_device(
    tokens, query_one, query_two, key_one, key_two, value_weight, mixing, out_weight, head_gain
):
    groups = lax.axis_size("tp")
    own_rows = tokens.shape[0]
    row_count = own_rows * groups
    head_cols = query_one.shape[1]
    head_local = head_cols // HEAD
    joined = jnp.concatenate([query_one, query_two, key_one, key_two, value_weight], axis=1)
    projected = jnp.dot(
        lax.all_gather(tokens, "tp", axis=0, tiled=True), joined, preferred_element_type=jnp.float32
    )
    positions = lax.axis_index("sp") * row_count + jnp.arange(row_count, dtype=jnp.int32)

    def heads_of(lower, upper):
        return projected[:, lower:upper].reshape(row_count, head_local, HEAD)

    q_first = grid_turn(heads_of(0, head_cols), positions).astype(jnp.bfloat16)
    q_second = grid_turn(heads_of(head_cols, 2 * head_cols), positions).astype(jnp.bfloat16)
    k_first = grid_turn(heads_of(2 * head_cols, 3 * head_cols), positions).astype(jnp.bfloat16)
    k_second = grid_turn(heads_of(3 * head_cols, 4 * head_cols), positions).astype(jnp.bfloat16)
    values = projected[:, 4 * head_cols :].astype(jnp.bfloat16)
    packed = jnp.concatenate(
        [k_first.reshape(row_count, head_cols), k_second.reshape(row_count, head_cols), values],
        axis=1,
    )
    absorb = make_absorb(q_first, q_second, head_local)
    empty = (
        jnp.full((row_count, head_local), floor_value, jnp.float32),
        jnp.zeros((row_count, head_local), jnp.float32),
        jnp.zeros((row_count, head_local, 2 * HEAD), jnp.float32),
    )
    gathered = lax.all_gather(packed, "sp", axis=0, tiled=True)
    first_map, second_map = absorb((empty, empty), gathered, 0)
    mixed = first_map[2] / first_map[1][..., None] - mixing[None, :, None] * (
        second_map[2] / second_map[1][..., None]
    )
    normed = (
        mixed * lax.rsqrt(jnp.mean(mixed * mixed, axis=-1, keepdims=True) + epsilon) * head_gain
    )
    heads = normed.astype(jnp.bfloat16).reshape(row_count, head_local * 2 * HEAD)
    regrouped = lax.all_to_all(heads, "tp", split_axis=0, concat_axis=1, tiled=True)
    summed = jnp.dot(regrouped, out_weight, preferred_element_type=jnp.float32)
    return summed.astype(jnp.bfloat16)


def solution(mesh):
    in_specs = (
        P(("sp", "tp"), None),
        P(None, "tp"),
        P(None, "tp"),
        P(None, "tp"),
        P(None, "tp"),
        P(None, "tp"),
        P("tp"),
        P(),
        P(),
    )
    out_specs = P(("sp", "tp"), None)
    return jax.shard_map(
        per_device, mesh=mesh, in_specs=in_specs, out_specs=out_specs, check_vma=False
    )
```

profile of v0, /device:TPU:0, one launch (start us, length us, event | category | flops | bytes accessed | tf_op | source)
XLA Modules:
  0.0 59.8 jit_solution(14919113349166023938)
XLA Ops:
  0.0 0.0 copy-start
  0.0 0.0 copy-start.1
  0.0 0.0 copy-start.2
  0.0 1.4 %copy.19 = bf16[2048,64]{1,0:T(8,128)(2,1)S(1)} copy(bf16[2048,64]{0,1:T(8,128)(2,1)} %param.10) | data formatting | bytes 524288 | tf_op args[1]
  1.4 2.0 %copy.20 = bf16[2048,64]{1,0:T(8,128)(2,1)} copy(bf16[2048,64]{0,1:T(8,128)(2,1)} %param.11) | data formatting | bytes 524288 | tf_op args[2]
  3.4 2.0 %copy.21 = bf16[2048,64]{1,0:T(8,128)(2,1)} copy(bf16[2048,64]{0,1:T(8,128)(2,1)} %param.12) | data formatting | bytes 524288 | tf_op args[3]
  5.3 0.0 copy-done.1
  5.3 1.0 %copy.22 = bf16[2048,64]{1,0:T(8,128)(2,1)} copy(bf16[2048,64]{0,1:T(8,128)(2,1)S(1)} %copy-done.1) | data formatting | bytes 524288 | tf_op args[4]
  6.4 0.0 copy-done.2
  6.4 8.6 %all_gather.6 = bf16[128,2048]{1,0:T(8,128)(2,1)S(1)} all-gather(bf16[32,2048]{1,0:T(8,128)(2,1)S(1)} %copy-done.2), channel_id=1, replica_groups=mesh['sp'=8,'tp'=4] {'tp'}, dimensions={0}, use_global_device_ids=true | all-gather | bytes 655360 | tf_op jit(solution)/shard_map/all_gather | solution.py:82
  15.0 4.1 %concatenate.63 = bf16[2048,384]{1,0:T(8,128)(2,1)} concatenate(bf16[2048,64]{1,0:T(8,128)(2,1)S(1)} %copy.19, bf16[2048,64]{1,0:T(8,128)(2,1)} %copy.20, bf16[2048,64]{1,0:T(8,128)(2,1)} %copy.21, bf16[2048,64]{1,0:T(8,128)(2,1)} %copy.22, bf16[2048,128]{1,0:T(8,128)(2,1)} %param.14), dimensions={1} | concatenate | bytes 3145728 | tf_op jit(solution)/shard_map/concatenate | solution.py:80
  19.1 2.0 %convolution_bitcast_fusion = f32[128,384]{0,1:T(8,128)S(1)} fusion(bf16[2048,384]{1,0:T(8,128)(2,1)} %concatenate.63, bf16[128,2048]{1,0:T(8,128)(2,1)S(1)} %all_gather.6), kind=kOutput, calls=%fused_computation.3 | convolution fusion | flops 201326592 | bytes 2293760 | tf_op jit(solution)/shard_map/dot_general | solution.py:81
  21.2 0.1 constant_dynamic-update-slice_fusion.7
  21.3 0.1 constant_dynamic-update-slice_fusion.6
  21.4 0.1 constant_dynamic-update-slice_fusion.5
  21.5 0.1 constant_dynamic-update-slice_fusion.4
  21.7 0.1 constant_dynamic-update-slice_fusion.3
  21.8 0.1 constant_dynamic-update-slice_fusion.2
  21.9 0.1 constant_dynamic-update-slice_fusion.1
  22.1 0.1 constant_dynamic-update-slice_fusion
  22.2 27.5 %all_gather.7 = bf16[1024,256]{0,1:T(8,128)(2,1)S(1)} all-gather(bf16[128,256]{0,1:T(8,128)(2,1)S(1)} %fusion.22), channel_id=1, replica_groups=mesh['sp'=8,'tp'=4] {'sp'}, dimensions={0}, use_global_device_ids=true | all-gather | bytes 589824 | tf_op jit(solution)/shard_map/all_gather | solution.py:104
  49.7 0.2 fusion.108
  49.8 0.0 copy-start.3
  49.8 0.3 fusion.117
  50.2 0.2 fusion.10
  51.0 0.3 fusion.118
  51.4 0.2 fusion.8
  51.5 0.3 fusion.5
  51.8 0.4 multiply_reduce_fusion
  52.2 0.0 copy-done.3
  52.2 0.1 multiply_convert_fusion
  52.3 6.3 %all_to_all.19 = bf16[4,32,128]{2,1,0:T(8,128)(2,1)S(1)} all-to-all(bf16[4,32,128]{2,1,0:T(8,128)(2,1)S(1)} %bitcast.110), channel_id=1, replica_groups=mesh['sp'=8,'tp'=4] {'tp'}, dimensions={0} | all-to-all | bytes 65536 | tf_op jit(solution)/shard_map/all_to_all | solution.py:113
  58.6 0.0 copy-done
  58.6 1.1 %convolution_convert_fusion = bf16[32,2048]{1,0:T(8,128)(2,1)} fusion(bf16[512,2048]{1,0:T(8,128)(2,1)S(1)} %copy-done, bf16[4,32,128]{2,1,0:T(8,128)(2,1)S(1)} %all_to_all.19), kind=kOutput, calls=%fused_computation | convolution fusion | flops 67174400 | bytes 2260992 | tf_op jit(solution)/shard_map/dot_general | solution.py:114
  (9 shorter events, 0.1 us)
Async XLA Ops:
  0.0 58.6 %copy-start = (bf16[512,2048]{1,0:T(8,128)(2,1)S(1)}, bf16[512,2048]{1,0:T(8,128)(2,1)}, u32[]{:S(2)}) copy-start(bf16[512,2048]{1,0:T(8,128)(2,1)} %param.16) | copy-start | bytes 6291460
  0.0 5.3 %copy-start.1 = (bf16[2048,64]{0,1:T(8,128)(2,1)S(1)}, bf16[2048,64]{0,1:T(8,128)(2,1)}, u32[]{:S(2)}) copy-start(bf16[2048,64]{0,1:T(8,128)(2,1)} %param.13) | copy-start | bytes 786436
  0.0 6.4 %copy-start.2 = (bf16[32,2048]{1,0:T(8,128)(2,1)S(1)}, bf16[32,2048]{1,0:T(8,128)(2,1)}, u32[]{:S(2)}) copy-start(bf16[32,2048]{1,0:T(8,128)(2,1)} %param.9) | copy-start | bytes 393220
  49.8 2.4 %copy-start.3 = (f32[128]{0:T(128)S(1)}, f32[128]{0:T(128)}, u32[]{:S(2)}) copy-start(f32[128]{0:T(128)} %param.17) | copy-start | bytes 1540
where the time goes:
time: 60.1 us; the launch traced here: 59.8 us
  blocking collectives  42.4 us (71%)
  local copies, waits for them, and re-layouts  10.5 us (17%)
  matrix products  4.48 us (7%)
  other arithmetic  1.64 us (3%)
  between operations  0.75 us (1%)
    all_gather x1, blocking collectives, per_device(): gathered = lax.all_gather(packed, 'sp', axis=0, tiled=True)  27.5 us
    all_gather x1, blocking collectives, per_device(): lax.all_gather(tokens, 'tp', axis=0, tiled=True)  8.64 us
    unnamed x12, local copies, waits for them, and re-layouts  6.35 us
    all_to_all x1, blocking collectives, per_device(): lax.all_to_all(heads, 'tp', split_axis=0, concat_axis=1, tiled=True)  6.3 us
    concatenate x1, local copies, waits for them, and re-layouts, per_device(): jnp.concatenate([query_one, query_two, key_one, key_two, value_weight], a...  4.1 us
    dot_general x1, matrix products, per_device(): jnp.dot(lax.all_gather(tokens, 'tp', axis=0, tiled=True), joined, preferr...  2.01 us

commit v1 on v0

--- a/solution.py
+++ b/solution.py
@@ -110,7 +110,9 @@
         mixed * lax.rsqrt(jnp.mean(mixed * mixed, axis=-1, keepdims=True) + epsilon) * head_gain
     )
     heads = normed.astype(jnp.bfloat16).reshape(row_count, head_local * 2 * HEAD)
-    regrouped = lax.all_to_all(heads, "tp", split_axis=0, concat_axis=1, tiled=True)
+    regrouped = jnp.concatenate(
+        lax.all_to_all(jnp.stack(jnp.split(heads, lax.axis_size("tp"), axis=0)), "tp", 0, 0), axis=1
+    )
     summed = jnp.dot(regrouped, out_weight, preferred_element_type=jnp.float32)
     return summed.astype(jnp.bfloat16)
 

time: 60.1 us -> 60.1 us (level)
  no operation moved by 1% of the time
where the time goes in v1:
time: 60.1 us; the launch traced here: 59.8 us
  blocking collectives  42.4 us (71%)
  local copies, waits for them, and re-layouts  10.5 us (17%)
  matrix products  4.48 us (7%)
  other arithmetic  1.65 us (3%)
  between operations  0.76 us (1%)
    all_gather x1, blocking collectives, per_device(): gathered = lax.all_gather(packed, 'sp', axis=0, tiled=True)  27.5 us
    all_gather x1, blocking collectives, per_device(): lax.all_gather(tokens, 'tp', axis=0, tiled=True)  8.64 us
    unnamed x12, local copies, waits for them, and re-layouts  6.35 us
    all_to_all x1, blocking collectives, per_device(): lax.all_to_all(jnp.stack(jnp.split(heads, lax.axis_size('tp'), axis=0)),...  6.3 us
    concatenate x1, local copies, waits for them, and re-layouts, per_device(): jnp.concatenate([query_one, query_two, key_one, key_two, value_weight], a...  4.1 us
    dot_general x1, matrix products, per_device(): jnp.dot(lax.all_gather(tokens, 'tp', axis=0, tiled=True), joined, preferr...  2.01 us

profile of v1, /device:TPU:0, one launch (start us, length us, event | category | flops | bytes accessed | tf_op | source)
XLA Modules:
  0.0 59.8 jit_solution(15953610616703112047)
XLA Ops:
  0.0 0.0 copy-start
  0.0 0.0 copy-start.1
  0.0 0.0 copy-start.2
  0.0 1.4 %copy.14 = bf16[2048,64]{1,0:T(8,128)(2,1)S(1)} copy(bf16[2048,64]{0,1:T(8,128)(2,1)} %param.10) | data formatting | bytes 524288 | tf_op args[1]
  1.4 2.0 %copy.15 = bf16[2048,64]{1,0:T(8,128)(2,1)} copy(bf16[2048,64]{0,1:T(8,128)(2,1)} %param.11) | data formatting | bytes 524288 | tf_op args[2]
  3.4 2.0 %copy.16 = bf16[2048,64]{1,0:T(8,128)(2,1)} copy(bf16[2048,64]{0,1:T(8,128)(2,1)} %param.12) | data formatting | bytes 524288 | tf_op args[3]
  5.3 0.0 copy-done.1
  5.3 1.0 %copy.17 = bf16[2048,64]{1,0:T(8,128)(2,1)} copy(bf16[2048,64]{0,1:T(8,128)(2,1)S(1)} %copy-done.1) | data formatting | bytes 524288 | tf_op args[4]
  6.4 0.0 copy-done.2
  6.4 8.6 %all_gather.6 = bf16[128,2048]{1,0:T(8,128)(2,1)S(1)} all-gather(bf16[32,2048]{1,0:T(8,128)(2,1)S(1)} %copy-done.2), channel_id=1, replica_groups=mesh['sp'=8,'tp'=4] {'tp'}, dimensions={0}, use_global_device_ids=true | all-gather | bytes 655360 | tf_op jit(solution)/shard_map/all_gather | solution.py:82
  15.0 4.1 %concatenate.63 = bf16[2048,384]{1,0:T(8,128)(2,1)} concatenate(bf16[2048,64]{1,0:T(8,128)(2,1)S(1)} %copy.14, bf16[2048,64]{1,0:T(8,128)(2,1)} %copy.15, bf16[2048,64]{1,0:T(8,128)(2,1)} %copy.16, bf16[2048,64]{1,0:T(8,128)(2,1)} %copy.17, bf16[2048,128]{1,0:T(8,128)(2,1)} %param.14), dimensions={1} | concatenate | bytes 3145728 | tf_op jit(solution)/shard_map/concatenate | solution.py:80
  19.1 2.0 %convolution_bitcast_fusion = f32[128,384]{0,1:T(8,128)S(1)} fusion(bf16[2048,384]{1,0:T(8,128)(2,1)} %concatenate.63, bf16[128,2048]{1,0:T(8,128)(2,1)S(1)} %all_gather.6), kind=kOutput, calls=%fused_computation.3 | convolution fusion | flops 201326592 | bytes 2293760 | tf_op jit(solution)/shard_map/dot_general | solution.py:81
  21.2 0.1 constant_dynamic-update-slice_fusion.7
  21.3 0.1 constant_dynamic-update-slice_fusion.6
  21.4 0.1 constant_dynamic-update-slice_fusion.5
  21.5 0.1 constant_dynamic-update-slice_fusion.4
  21.7 0.1 constant_dynamic-update-slice_fusion.3
  21.8 0.1 constant_dynamic-update-slice_fusion.2
  21.9 0.1 constant_dynamic-update-slice_fusion.1
  22.1 0.1 constant_dynamic-update-slice_fusion
  22.2 27.5 %all_gather.7 = bf16[1024,256]{0,1:T(8,128)(2,1)S(1)} all-gather(bf16[128,256]{0,1:T(8,128)(2,1)S(1)} %fusion.23), channel_id=1, replica_groups=mesh['sp'=8,'tp'=4] {'sp'}, dimensions={0}, use_global_device_ids=true | all-gather | bytes 589824 | tf_op jit(solution)/shard_map/all_gather | solution.py:104
  49.7 0.2 fusion.109
  49.8 0.0 copy-start.3
  49.8 0.3 fusion.118
  50.2 0.2 fusion.10
  51.0 0.3 fusion.119
  51.4 0.2 fusion.8
  51.5 0.3 fusion.5
  51.8 0.4 multiply_reduce_fusion
  52.2 0.0 copy-done.3
  52.2 0.1 fusion.22
  52.3 6.3 %all_to_all.5 = bf16[4,32,128]{2,1,0:T(8,128)(2,1)S(1)} all-to-all(bf16[4,32,128]{2,1,0:T(8,128)(2,1)S(1)} %pad_maximum_fusion), channel_id=1, replica_groups=mesh['sp'=8,'tp'=4] {'tp'}, dimensions={0} | all-to-all | bytes 65536 | tf_op jit(solution)/shard_map/all_to_all | solution.py:114
  58.6 0.0 copy-done
  58.6 1.1 %convolution_convert_fusion = bf16[32,2048]{1,0:T(8,128)(2,1)} fusion(bf16[512,2048]{1,0:T(8,128)(2,1)S(1)} %copy-done, bf16[4,32,128]{2,1,0:T(8,128)(2,1)S(1)} %all_to_all.5), kind=kOutput, calls=%fused_computation | convolution fusion | flops 67174400 | bytes 2260992 | tf_op jit(solution)/shard_map/dot_general | solution.py:116
  (11 shorter events, 0.1 us)
Async XLA Ops:
  0.0 58.6 %copy-start = (bf16[512,2048]{1,0:T(8,128)(2,1)S(1)}, bf16[512,2048]{1,0:T(8,128)(2,1)}, u32[]{:S(2)}) copy-start(bf16[512,2048]{1,0:T(8,128)(2,1)} %param.16) | copy-start | bytes 6291460
  0.0 5.3 %copy-start.1 = (bf16[2048,64]{0,1:T(8,128)(2,1)S(1)}, bf16[2048,64]{0,1:T(8,128)(2,1)}, u32[]{:S(2)}) copy-start(bf16[2048,64]{0,1:T(8,128)(2,1)} %param.13) | copy-start | bytes 786436
  0.0 6.4 %copy-start.2 = (bf16[32,2048]{1,0:T(8,128)(2,1)S(1)}, bf16[32,2048]{1,0:T(8,128)(2,1)}, u32[]{:S(2)}) copy-start(bf16[32,2048]{1,0:T(8,128)(2,1)} %param.9) | copy-start | bytes 393220
  49.8 2.4 %copy-start.3 = (f32[128]{0:T(128)S(1)}, f32[128]{0:T(128)}, u32[]{:S(2)}) copy-start(f32[128]{0:T(128)} %param.17) | copy-start | bytes 1540
